TPU v7x, 32 devices: a whole 2x2x4 slice. The times are simulated.
32 devices in a mesh: tp: 32 (over z, y, x, core).
Axes of the slice: x: 2, y: 2, z: 4, core: 2. Of those that a mesh axis runs over, the one named last changes fastest.
Arguments:
- tokens: bfloat16 [32, 4096], replicated, may hold values from -18 to 18
- norm_gain: float32 [2, 4096], replicated, may hold values from 0.1 to 1.9
- w_gate: bfloat16 [2, 4096, 8192], P(None, None, 'tp'), may hold values from -0.09375 to 0.09375
- w_value: bfloat16 [2, 4096, 8192], P(None, None, 'tp'), may hold values from -0.09375 to 0.09375
- w_write: bfloat16 [2, 4096, 1024], P(None, None, 'tp'), may hold values from -0.09375 to 0.09375
- w_read: bfloat16 [2, 4096, 1024], P(None, None, 'tp'), may hold values from -0.09375 to 0.09375
- w_step: bfloat16 [2, 4096, 128], replicated, may hold values from -0.09375 to 0.09375
- step_bias: float32 [2, 128], replicated, may hold values from -2 to 1
- decay_rate: float32 [2, 128], replicated, may hold values from 0.05 to 3
- skip_gain: float32 [2, 128], replicated, may hold values from 1 to 4
- conv_value_weight: float32 [2, 3, 8192], P(None, None, 'tp'), may hold values from -2.5 to 2.5
- conv_key_weight: float32 [2, 3, 2, 1024], P(None, None, None, 'tp'), may hold values from -2.5 to 2.5
- group_gain: float32 [2, 8192], P(None, 'tp'), may hold values from 0.1 to 1.9
- w_out: bfloat16 [2, 8192, 4096], P(None, 'tp'), may hold values from -0.0625 to 0.0625
- ssm_state: float32 [2, 32, 8192, 128], P(None, None, 'tp'), may hold values from -3 to 3
- conv_value: float32 [2, 32, 2, 8192], P(None, None, None, 'tp'), may hold values from -5 to 5
- conv_key: float32 [2, 32, 2, 2, 1024], P(None, None, None, None, 'tp'), may hold values from -5 to 5
Outputs:
- tokens_out: bfloat16 [32, 4096], replicated
- ssm_state_out: float32 [2, 32, 8192, 128], P(None, None, 'tp')
- conv_value_out: float32 [2, 32, 2, 8192], P(None, None, None, 'tp')
- conv_key_out: float32 [2, 32, 2, 2, 1024], P(None, None, None, None, 'tp')
All inputs are finite; a program needn't handle non-finite values.
Results may differ from a plain program's by a relative error of at most 0.011.
Values may be sent and summed in bfloat16 or wider, within the bound.
A program may use at most 128 MiB of HBM per device.

v0:
```python
import jax
import jax.numpy as jnp
from jax import lax
from jax.sharding import PartitionSpec as P

D = 4096
HEAD_DIM = 64
GROUPS = 8
STATE = 128
LAYERS = 2
HEADS = 128
GW = 1024
EPS = 1e-06


def per_device(
    tokens,
    norm_gain,
    w_gate,
    w_value,
    w_write,
    w_read,
    w_step,
    step_bias,
    decay_rate,
    skip_gain,
    conv_value_weight,
    conv_key_weight,
    group_gain,
    w_out,
    ssm_state,
    conv_value,
    conv_key,
):
    highest = lax.Precision.HIGHEST
    chan_count = w_gate.shape[2]
    position = lax.axis_index("tp")
    first_chan = position * chan_count
    chan_ids = first_chan + jnp.arange(chan_count, dtype=jnp.int32)
    my_group = first_chan // GW
    head_hot = (
        (chan_ids // HEAD_DIM)[:, None] == jnp.arange(HEADS, dtype=jnp.int32)[None, :]
    ).astype(jnp.float32)
    group_hot = ((chan_ids // GW)[:, None] == jnp.arange(GROUPS, dtype=jnp.int32)[None, :]).astype(
        jnp.float32
    )
    hidden = tokens
    ssm_list = []
    value_list = []
    key_list = []
    for layer in range(LAYERS):
        resid = hidden.astype(jnp.float32)
        inv_scale = lax.rsqrt(jnp.sum(resid * resid, axis=1) / D + EPS)[:, None]
        scaled = (resid * norm_gain[layer]).astype(jnp.bfloat16)

        def project(weight):
            return jnp.dot(scaled, weight[layer], preferred_element_type=jnp.float32) * inv_scale

        gate_in = project(w_gate)
        value_in = project(w_value)
        write_in = project(w_write)
        read_in = project(w_read)
        step_in = project(w_step)
        value_window = jnp.concatenate([conv_value[layer], value_in[:, None, :]], axis=1)
        value_list.append(value_window[:, 1:])
        values = jax.nn.silu(jnp.sum(value_window * conv_value_weight[layer][None], axis=1))
        fresh = jnp.stack([write_in, read_in], axis=1)[:, None]
        key_window = jnp.concatenate([conv_key[layer], fresh], axis=1)
        key_list.append(key_window[:, 1:])
        mixed_keys = jax.nn.silu(jnp.sum(key_window * conv_key_weight[layer][None], axis=1))
        every_group = lax.all_gather(mixed_keys, "tp", axis=2, tiled=True)
        by_entry = every_group.reshape(every_group.shape[0], 2, STATE, GROUPS)
        own_keys = lax.dynamic_slice_in_dim(by_entry, my_group, 1, 3)[..., 0]
        writes = own_keys[:, 0]
        reads = own_keys[:, 1]
        delta = jax.nn.softplus(step_in + step_bias[layer][None])
        decay = jnp.exp(-delta * decay_rate[layer][None])
        delta_chan = jnp.dot(delta, head_hot.T, precision=highest)
        decay_chan = jnp.dot(decay, head_hot.T, precision=highest)
        skip_chan = jnp.dot(skip_gain[layer], head_hot.T, precision=highest)
        state = (
            decay_chan[..., None] * ssm_state[layer]
            + (delta_chan * values)[..., None] * writes[:, None, :]
        )
        ssm_list.append(state)
        read_out = jnp.sum(state * reads[:, None, :], axis=2) + skip_chan[None] * values
        gated = read_out * jax.nn.silu(gate_in)
        squares = jnp.dot(gated * gated, group_hot, precision=highest)
        square_total = lax.psum(squares, "tp")
        group_scale = lax.rsqrt(square_total / GW + EPS)
        scale_chan = jnp.dot(group_scale, group_hot.T, precision=highest)
        normed = (gated * scale_chan * group_gain[layer][None]).astype(jnp.bfloat16)
        partial_out = jnp.dot(normed, w_out[layer], preferred_element_type=jnp.float32)
        update = lax.psum(partial_out, "tp")
        hidden = (resid + update).astype(jnp.bfloat16)
    return (hidden, jnp.stack(ssm_list), jnp.stack(value_list), jnp.stack(key_list))


def solution(mesh):
    placed = (
        P(),
        P(),
        P(None, None, "tp"),
        P(None, None, "tp"),
        P(None, None, "tp"),
        P(None, None, "tp"),
        P(),
        P(),
        P(),
        P(),
        P(None, None, "tp"),
        P(None, None, None, "tp"),
        P(None, "tp"),
        P(None, "tp", None),
        P(None, None, "tp", None),
        P(None, None, None, "tp"),
        P(None, None, None, None, "tp"),
    )
    return jax.shard_map(
        per_device,
        mesh=mesh,
        in_specs=placed,
        out_specs=(
            P(),
            P(None, None, "tp", None),
            P(None, None, None, "tp"),
            P(None, None, None, None, "tp"),
        ),
        check_vma=False,
    )
```

profile of v0, /device:TPU:0, one launch (start us, length us, event | category | flops | bytes accessed | tf_op | source)
XLA Modules:
  0.0 486.0 jit_solution(18059725305354858468)
XLA Ops:
  7.3 1.3 fusion.57
  8.6 0.8 slice_bitcast_fusion.11
  10.1 0.8 fusion.160
  10.9 0.8 fusion.159
  12.3 0.9 fusion.158
  13.2 1.2 fusion.51
  14.4 1.2 fusion.50
  15.8 2.1 fusion.29
  19.3 46.2 %all_gather.6 = f32[32,2,1024]{0,1,2:T(2,128)S(1)} all-gather(f32[32,2,32]{0,1,2:T(2,128)S(1)} %copy.61), channel_id=1, replica_groups=mesh['tp'=32] {'tp'}, dimensions={2}, use_global_device_ids=true | all-gather | bytes 270336 | tf_op jit(solution)/shard_map/all_gather | solution.py:71
  65.8 5.5 %fusion.5 = f32[32,256]{1,0:T(8,128)S(1)} fusion(f32[2,32,256,128]{3,2,1,0:T(8,128)} %param.31, f32[32,128]{1,0:T(8,128)S(1)} %get-tuple-element.17, f32[32,128]{1,0:T(8,128)S(1)} %get-tuple-element.16, f32[32,256]{1,0:T(8,128)S(1)} %convolution_multiply_fusion.3, f32[32,256]{1,0:T(8,128)S(1)} %fusion.79), kind=kLoop, calls=%fused_computation.8 | loop fusion | flops 5234688 | bytes 4325376 | tf_op jit(solution)/shard_map/reduce_sum | solution.py:86
  72.1 36.8 %psum.28 = f32[32,8]{0,1:T(8,128)S(1)} all-reduce(f32[32,8]{0,1:T(8,128)S(1)} %fusion.75), channel_id=1, replica_groups=mesh['tp'=32] {'tp'}, use_global_device_ids=true, to_apply=%region_4.5 | all-reduce | flops 256 | bytes 2048 | tf_op jit(solution)/shard_map/psum | solution.py:89
  109.2 2.9 fusion.12
  112.4 129.4 %all-reduce.3.cloned.1.call-done = f32[32,4096]{1,0:T(8,128)} async-done(((f32[32,4096]{1,0:T(8,128)}), f32[32,4096]{1,0:T(8,128)}) %all-reduce.3.cloned.1.call-update) | async-done | bytes 524304 | tf_op jit(solution)/shard_map/psum | solution.py:94
  241.8 1.2 fusion.60
  243.5 2.0 fusion.38
  245.5 1.5 compare_select_fusion
  248.1 42.5 %all_gather.7 = f32[32,2,1024]{0,1,2:T(2,128)S(1)} all-gather(f32[32,2,32]{0,1,2:T(2,128)S(1)} %copy.68), channel_id=1, replica_groups=mesh['tp'=32] {'tp'}, dimensions={2}, use_global_device_ids=true | all-gather | bytes 270336 | tf_op jit(solution)/shard_map/all_gather | solution.py:71
  290.9 10.5 %multiply_add_fusion.1 = (f32[1,32,256,128]{3,2,1,0:T(8,128)}, f32[1,32,256,128]{3,2,1,0:T(8,128)}) fusion(f32[2,32,256,128]{3,2,1,0:T(8,128)} %param.31, f32[32,128]{1,0:T(8,128)S(1)} %get-tuple-element.16, f32[32,256]{1,0:T(8,128)S(1)} %convolution_multiply_fusion.3, f32[32,256]{1,0:T(8,128)S(1)} %fusion.79, f32[32,128]{1,0:T(8,128)S(1)} %get-tuple-element.12, ...), kind=kLoop, calls=%fused_computation.10 | loop fusion | flops 6291456 | bytes 16941056 | tf_op jit(solution)/shard_map/add | solution.py:82
  301.4 5.5 %fusion.2 = f32[32,256]{1,0:T(8,128)S(1)} fusion(f32[2,32,256,128]{3,2,1,0:T(8,128)} %param.31, f32[32,128]{1,0:T(8,128)S(1)} %get-tuple-element.13, f32[32,128]{1,0:T(8,128)S(1)} %get-tuple-element.12, f32[32,256]{1,0:T(8,128)S(1)} %convolution_multiply_fusion.1, f32[32,256]{1,0:T(8,128)S(1)} %fusion.78), kind=kLoop, calls=%fused_computation.4 | loop fusion | flops 5234688 | bytes 4325376 | tf_op jit(solution)/shard_map/reduce_sum | solution.py:86
  307.6 36.8 %psum.30 = f32[32,8]{0,1:T(8,128)S(1)} all-reduce(f32[32,8]{0,1:T(8,128)S(1)} %fusion.74), channel_id=1, replica_groups=mesh['tp'=32] {'tp'}, use_global_device_ids=true, to_apply=%region_10.11 | all-reduce | flops 256 | bytes 2048 | tf_op jit(solution)/shard_map/psum | solution.py:89
  344.7 2.9 fusion.6
  349.1 7.9 %pad_maximum_fusion = f32[2,32,256,128]{3,2,1,0:T(8,128)} fusion(f32[1,32,256,128]{3,2,1,0:T(8,128)} %get-tuple-element.7, f32[1,32,256,128]{3,2,1,0:T(8,128)} %get-tuple-element.6), kind=kLoop, calls=%fused_computation | loop fusion | flops 2097152 | bytes 16777216 | tf_op jit(solution)/shard_map/stack | solution.py:96
  357.0 120.4 %all-reduce.5.cloned.1.call-done = f32[32,4096]{1,0:T(8,128)} async-done(((f32[32,4096]{1,0:T(8,128)}), f32[32,4096]{1,0:T(8,128)}) %all-reduce.5.cloned.1.call-update) | async-done | bytes 524304 | tf_op jit(solution)/shard_map/psum | solution.py:94
  477.4 1.8 fusion.61
  (74 shorter events, 8.7 us)
Async XLA Ops:
  7.2 10.9 %copy-start = (bf16[32,4096]{1,0:T(8,128)(2,1)S(1)}, bf16[32,4096]{1,0:T(8,128)(2,1)}, u32[]{:S(2)}) copy-start(bf16[32,4096]{1,0:T(8,128)(2,1)} %param.17) | copy-start | bytes 786436
  7.2 10.7 %copy-start.1 = (f32[2,32,2,256]{3,2,1,0:T(2,128)S(1)}, f32[2,32,2,256]{3,2,1,0:T(2,128)}, u32[]{:S(2)}) copy-start(f32[2,32,2,256]{3,2,1,0:T(2,128)} %param.32) | copy-start | bytes 393220
  7.2 10.8 %copy-start.8 = (f32[2,128]{1,0:T(2,128)S(1)}, f32[2,128]{1,0:T(2,128)}, u32[]{:S(2)}) copy-start(f32[2,128]{1,0:T(2,128)} %param.26) | copy-start | bytes 3076
  7.2 11.9 %copy-start.2 = (f32[2,32,2,2,32]{4,3,2,1,0:T(2,128)S(1)}, f32[2,32,2,2,32]{4,3,2,1,0:T(2,128)}, u32[]{:S(2)}) copy-start(f32[2,32,2,2,32]{4,3,2,1,0:T(2,128)} %param.33) | copy-start | bytes 98308
  7.2 234.6 %all-reduce.3.cloned.1.call-start = ((), (), s32[]{:S(2)}) async-start(), calls=%async_computation | async-start | bytes 1048576 | tf_op jit(solution)/shard_map/psum | solution.py:94
  7.3 10.8 %copy-start.5 = (bf16[2,4096,128]{2,1,0:T(8,128)(2,1)S(1)}, bf16[2,4096,128]{2,1,0:T(8,128)(2,1)}, u32[]{:S(2)}) copy-start(bf16[2,4096,128]{2,1,0:T(8,128)(2,1)} %param.23) | copy-start | bytes 6291460
  65.8 5.6 %copy-start.3 = (bf16[2,4096,256]{2,1,0:T(8,128)(2,1)S(1)}, bf16[2,4096,256]{2,1,0:T(8,128)(2,1)}, u32[]{:S(2)}) copy-start(bf16[2,4096,256]{2,1,0:T(8,128)(2,1)} %param.19) | copy-start | bytes 12582916
  71.3 171.7 %copy-start.6 = (bf16[2,4096,32]{1,2,0:T(8,128)(2,1)S(1)}, bf16[2,4096,32]{1,2,0:T(8,128)(2,1)}, u32[]{:S(2)}) copy-start(bf16[2,4096,32]{1,2,0:T(8,128)(2,1)} %param.22) | copy-start | bytes 1572868
  71.3 171.9 %copy-start.7 = (bf16[2,4096,32]{1,2,0:T(8,128)(2,1)S(1)}, bf16[2,4096,32]{1,2,0:T(8,128)(2,1)}, u32[]{:S(2)}) copy-start(bf16[2,4096,32]{1,2,0:T(8,128)(2,1)} %param.21) | copy-start | bytes 1572868
  112.1 365.3 %all-reduce.5.cloned.1.call-start = ((), (), s32[]{:S(2)}) async-start(), calls=%async_computation.1 | async-start | bytes 1048576 | tf_op jit(solution)/shard_map/psum | solution.py:94
  301.4 5.5 %copy-start.4 = (bf16[2,4096,256]{2,1,0:T(8,128)(2,1)S(1)}, bf16[2,4096,256]{2,1,0:T(8,128)(2,1)}, u32[]{:S(2)}) copy-start(bf16[2,4096,256]{2,1,0:T(8,128)(2,1)} %param.19) | copy-start | bytes 12582916
Sparse Core Ops, SparseCore 0:
  112.2 129.5 all-reduce.2
  347.8 129.4 all-reduce.4
where the time goes:
time: 487 us; the launch traced here: 486 us
  waiting for transfers between devices  250 us (51%)
  blocking collectives  162 us (33%)
  other arithmetic  35.8 us (7%)
  matrix products  18 us (4%)
  between operations  14.5 us (3%)
  local copies, waits for them, and re-layouts  5.49 us (1%)
    psum x2, waiting for transfers between devices, per_device(): update = lax.psum(partial_out, 'tp')  250 us
    all_gather x2, blocking collectives, per_device(): every_group = lax.all_gather(mixed_keys, 'tp', axis=2, tiled=True)  88.7 us
    psum x2, blocking collectives, per_device(): square_total = lax.psum(squares, 'tp')  73.6 us
    reduce_sum x2, other arithmetic, per_device(): jnp.sum(state * reads[:, None, :], axis=2) + skip_chan[None] * values  11 us
    add x1, other arithmetic, per_device(): decay_chan[..., None] * ssm_state[layer]  10.5 us
  transfers between devices with their start and end apart: 2, of which 2 were waited for; matrix products, arithmetic and copies ran while one was open for 2% of the time, Pallas kernels for 0%

commit v1 on v0

--- a/solution.py
+++ b/solution.py
@@ -91,7 +91,9 @@
         scale_chan = jnp.dot(group_scale, group_hot.T, precision=highest)
         normed = (gated * scale_chan * group_gain[layer][None]).astype(jnp.bfloat16)
         partial_out = jnp.dot(normed, w_out[layer], preferred_element_type=jnp.float32)
-        update = lax.psum(partial_out, "tp")
+        update = partial_out
+        for hop in (1, 2, 4, 8, 16):
+            update = update + lax.ppermute(update, "tp", [(dev, dev ^ hop) for dev in range(32)])
         hidden = (resid + update).astype(jnp.bfloat16)
     return (hidden, jnp.stack(ssm_list), jnp.stack(value_list), jnp.stack(key_list))
 

time: 487 us -> 332 us (0.68)
  waiting for transfers between devices: 250 us -> 104 us
  starting transfers between devices: 0.08 us -> 18 us
  between operations: 14.5 us -> 1.2 us
  other arithmetic: 35.8 us -> 28.1 us
    psum x2 -> x0, waiting for transfers between devices: 250 us -> none  [per_device(): update = lax.psum(partial_out, 'tp')]
    ppermute x0 -> x10, waiting for transfers between devices: none -> 104 us  [per_device(): lax.ppermute(update, 'tp', [(dev, dev ^ hop) for dev in range(32)])]
    ppermute x0 -> x10, starting transfers between devices: none -> 18 us  [per_device(): lax.ppermute(update, 'tp', [(dev, dev ^ hop) for dev in range(32)])]
  transfers between devices with their start and end apart: 2 -> 10, of which waited for: 2 -> 10; matrix products, arithmetic and copies ran while one was open for 2% -> 4% of each run, Pallas kernels for 0% -> 0%
where the time goes in v1:
time: 332 us; the launch traced here: 331 us
  blocking collectives  161 us (48%)
  waiting for transfers between devices  104 us (31%)
  other arithmetic  28.1 us (8%)
  starting transfers between devices  18 us (5%)
  matrix products  13.5 us (4%)
  local copies, waits for them, and re-layouts  5.52 us (2%)
    ppermute x10, waiting for transfers between devices, per_device(): lax.ppermute(update, 'tp', [(dev, dev ^ hop) for dev in range(32)])  104 us
    all_gather x2, blocking collectives, per_device(): every_group = lax.all_gather(mixed_keys, 'tp', axis=2, tiled=True)  87.1 us
    psum x2, blocking collectives, per_device(): square_total = lax.psum(squares, 'tp')  73.6 us
    ppermute x10, starting transfers between devices, per_device(): lax.ppermute(update, 'tp', [(dev, dev ^ hop) for dev in range(32)])  18 us
    reduce_sum x2, other arithmetic, per_device(): jnp.sum(state * reads[:, None, :], axis=2) + skip_chan[None] * values  11.1 us
    add x1, other arithmetic, per_device(): decay_chan[..., None] * ssm_state[layer]  8.16 us
    dot_general x10, matrix products, project(): jnp.dot(scaled, weight[layer], preferred_element_type=jnp.float32)  6.84 us
  transfers between devices with their start and end apart: 10, of which 10 were waited for; matrix products, arithmetic and copies ran while one was open for 4% of the time, Pallas kernels for 0%

profile of v1, /device:TPU:0, one launch (start us, length us, event | category | flops | bytes accessed | tf_op | source)
XLA Modules:
  0.0 330.7 jit_solution(9037258707302722763)
XLA Ops:
  9.2 2.1 fusion.29
  12.8 46.2 %all_gather.6 = f32[32,2,1024]{0,1,2:T(2,128)S(1)} all-gather(f32[32,2,32]{0,1,2:T(2,128)S(1)} %copy.61), channel_id=1, replica_groups=mesh['tp'=32] {'tp'}, dimensions={2}, use_global_device_ids=true | all-gather | bytes 270336 | tf_op jit(solution)/shard_map/all_gather | solution.py:71
  59.2 5.5 %fusion.5 = f32[32,256]{1,0:T(8,128)S(1)} fusion(f32[2,32,256,128]{3,2,1,0:T(8,128)} %param.31, f32[32,128]{1,0:T(8,128)S(1)} %get-tuple-element.17, f32[32,128]{1,0:T(8,128)S(1)} %get-tuple-element.16, f32[32,256]{1,0:T(8,128)S(1)} %convolution_multiply_fusion.3, f32[32,256]{1,0:T(8,128)S(1)} %fusion.79), kind=kLoop, calls=%fused_computation.8 | loop fusion | flops 5234688 | bytes 4325376 | tf_op jit(solution)/shard_map/reduce_sum | solution.py:86
  65.5 36.8 %psum.14 = f32[32,8]{0,1:T(8,128)S(1)} all-reduce(f32[32,8]{0,1:T(8,128)S(1)} %fusion.75), channel_id=1, replica_groups=mesh['tp'=32] {'tp'}, use_global_device_ids=true, to_apply=%region_4.5 | all-reduce | flops 256 | bytes 2048 | tf_op jit(solution)/shard_map/psum | solution.py:89
  102.6 2.0 fusion.12
  104.8 1.9 collective-permute-done
  106.8 2.3 collective-permute-start.1
  109.1 12.2 %collective-permute-done.1 = f32[32,4096]{1,0:T(8,128)S(1)} collective-permute-done((f32[32,4096]{1,0:T(8,128)S(1)}, f32[32,4096]{1,0:T(8,128)S(1)}, u32[]{:S(2)}, u32[]{:S(2)}) %collective-permute-start.1) | collective-permute-done | bytes 524320 | tf_op jit(solution)/shard_map/ppermute | solution.py:96
  123.2 11.7 %collective-permute-done.2 = f32[32,4096]{1,0:T(8,128)S(1)} collective-permute-done((f32[32,4096]{1,0:T(8,128)S(1)}, f32[32,4096]{1,0:T(8,128)S(1)}, u32[]{:S(2)}, u32[]{:S(2)}) %collective-permute-start.2) | collective-permute-done | bytes 524320 | tf_op jit(solution)/shard_map/ppermute | solution.py:96
  134.9 2.9 collective-permute-start.3
  137.9 10.8 %collective-permute-done.3 = f32[32,4096]{1,0:T(8,128)S(1)} collective-permute-done((f32[32,4096]{1,0:T(8,128)S(1)}, f32[32,4096]{1,0:T(8,128)S(1)}, u32[]{:S(2)}, u32[]{:S(2)}) %collective-permute-start.3) | collective-permute-done | bytes 524320 | tf_op jit(solution)/shard_map/ppermute | solution.py:96
  150.7 22.1 %collective-permute-done.4 = f32[32,4096]{1,0:T(8,128)S(1)} collective-permute-done((f32[32,4096]{1,0:T(8,128)S(1)}, f32[32,4096]{1,0:T(8,128)S(1)}, u32[]{:S(2)}, u32[]{:S(2)}) %collective-permute-start.4) | collective-permute-done | bytes 524320 | tf_op jit(solution)/shard_map/ppermute | solution.py:96
  175.3 40.9 %all_gather.7 = f32[32,2,1024]{0,1,2:T(2,128)S(1)} all-gather(f32[32,2,32]{0,1,2:T(2,128)S(1)} %copy.68), channel_id=1, replica_groups=mesh['tp'=32] {'tp'}, dimensions={2}, use_global_device_ids=true | all-gather | bytes 270336 | tf_op jit(solution)/shard_map/all_gather | solution.py:71
  216.4 5.5 %fusion.2 = f32[32,256]{1,0:T(8,128)S(1)} fusion(f32[2,32,256,128]{3,2,1,0:T(8,128)} %param.31, f32[32,128]{1,0:T(8,128)S(1)} %get-tuple-element.13, f32[32,128]{1,0:T(8,128)S(1)} %get-tuple-element.12, f32[32,256]{1,0:T(8,128)S(1)} %convolution_multiply_fusion.1, f32[32,256]{1,0:T(8,128)S(1)} %fusion.78), kind=kLoop, calls=%fused_computation.4 | loop fusion | flops 5234688 | bytes 4325376 | tf_op jit(solution)/shard_map/reduce_sum | solution.py:86
  222.7 36.8 %psum.15 = f32[32,8]{0,1:T(8,128)S(1)} all-reduce(f32[32,8]{0,1:T(8,128)S(1)} %fusion.74), channel_id=1, replica_groups=mesh['tp'=32] {'tp'}, use_global_device_ids=true, to_apply=%region_9.10 | all-reduce | flops 256 | bytes 2048 | tf_op jit(solution)/shard_map/psum | solution.py:89
  259.8 2.1 fusion.6
  263.9 2.3 collective-permute-start.6
  266.2 12.2 %collective-permute-done.6 = f32[32,4096]{1,0:T(8,128)S(1)} collective-permute-done((f32[32,4096]{1,0:T(8,128)S(1)}, f32[32,4096]{1,0:T(8,128)S(1)}, u32[]{:S(2)}, u32[]{:S(2)}) %collective-permute-start.6) | collective-permute-done | bytes 524320 | tf_op jit(solution)/shard_map/ppermute | solution.py:96
  281.2 10.8 %collective-permute-done.7 = f32[32,4096]{1,0:T(8,128)S(1)} collective-permute-done((f32[32,4096]{1,0:T(8,128)S(1)}, f32[32,4096]{1,0:T(8,128)S(1)}, u32[]{:S(2)}, u32[]{:S(2)}) %collective-permute-start.7) | collective-permute-done | bytes 524320 | tf_op jit(solution)/shard_map/ppermute | solution.py:96
  292.0 2.9 collective-permute-start.8
  295.0 8.2 %multiply_add_fusion.1 = (f32[1,32,256,128]{3,2,1,0:T(8,128)S(1)}, f32[1,32,256,128]{3,2,1,0:T(8,128)S(1)}) fusion(f32[2,32,256,128]{3,2,1,0:T(8,128)} %param.31, f32[32,128]{1,0:T(8,128)S(1)} %get-tuple-element.16, f32[32,256]{1,0:T(8,128)S(1)} %convolution_multiply_fusion.3, f32[32,256]{1,0:T(8,128)S(1)} %fusion.79, f32[32,128]{1,0:T(8,128)S(1)} %get-tuple-element.12, ...), kind=kLoop, calls=%fused_computation.10 | loop fusion | flops 6291456 | bytes 16941056 | tf_op jit(solution)/shard_map/add | solution.py:82
  303.1 2.6 collective-permute-done.8
  308.5 3.9 %pad_maximum_fusion = f32[2,32,256,128]{3,2,1,0:T(8,128)} fusion(f32[1,32,256,128]{3,2,1,0:T(8,128)S(1)} %get-tuple-element.7, f32[1,32,256,128]{3,2,1,0:T(8,128)S(1)} %get-tuple-element.6), kind=kLoop, calls=%fused_computation | loop fusion | flops 2097152 | bytes 16777216 | tf_op jit(solution)/shard_map/stack | solution.py:98
  312.4 17.5 %collective-permute-done.9 = f32[32,4096]{1,0:T(8,128)S(1)} collective-permute-done((f32[32,4096]{1,0:T(8,128)S(1)}, f32[32,4096]{1,0:T(8,128)S(1)}, u32[]{:S(2)}, u32[]{:S(2)}) %collective-permute-start.9) | collective-permute-done | bytes 524320 | tf_op jit(solution)/shard_map/ppermute | solution.py:96
  (100 shorter events, 27.1 us)
Async XLA Ops:
  0.6 10.9 %copy-start = (bf16[32,4096]{1,0:T(8,128)(2,1)S(1)}, bf16[32,4096]{1,0:T(8,128)(2,1)}, u32[]{:S(2)}) copy-start(bf16[32,4096]{1,0:T(8,128)(2,1)} %param.17) | copy-start | bytes 786436
  0.6 10.7 %copy-start.1 = (f32[2,32,2,256]{3,2,1,0:T(2,128)S(1)}, f32[2,32,2,256]{3,2,1,0:T(2,128)}, u32[]{:S(2)}) copy-start(f32[2,32,2,256]{3,2,1,0:T(2,128)} %param.32) | copy-start | bytes 393220
  0.7 10.7 %copy-start.10 = (f32[2,128]{1,0:T(2,128)S(1)}, f32[2,128]{1,0:T(2,128)}, u32[]{:S(2)}) copy-start(f32[2,128]{1,0:T(2,128)} %param.26) | copy-start | bytes 3076
  0.7 10.9 %copy-start.6 = (bf16[2,4096,128]{2,1,0:T(8,128)(2,1)S(1)}, bf16[2,4096,128]{2,1,0:T(8,128)(2,1)}, u32[]{:S(2)}) copy-start(bf16[2,4096,128]{2,1,0:T(8,128)(2,1)} %param.23) | copy-start | bytes 6291460
  0.7 11.9 %copy-start.2 = (f32[2,32,2,2,32]{4,3,2,1,0:T(2,128)S(1)}, f32[2,32,2,2,32]{4,3,2,1,0:T(2,128)}, u32[]{:S(2)}) copy-start(f32[2,32,2,2,32]{4,3,2,1,0:T(2,128)} %param.33) | copy-start | bytes 98308
  59.2 5.6 %copy-start.4 = (bf16[2,4096,256]{2,1,0:T(8,128)(2,1)S(1)}, bf16[2,4096,256]{2,1,0:T(8,128)(2,1)}, u32[]{:S(2)}) copy-start(bf16[2,4096,256]{2,1,0:T(8,128)(2,1)} %param.19) | copy-start | bytes 12582916
  104.7 68.4 %copy-start.8 = (bf16[2,4096,32]{1,2,0:T(8,128)(2,1)S(1)}, bf16[2,4096,32]{1,2,0:T(8,128)(2,1)}, u32[]{:S(2)}) copy-start(bf16[2,4096,32]{1,2,0:T(8,128)(2,1)} %param.22) | copy-start | bytes 1572868
  104.7 68.6 %copy-start.9 = (bf16[2,4096,32]{1,2,0:T(8,128)(2,1)S(1)}, bf16[2,4096,32]{1,2,0:T(8,128)(2,1)}, u32[]{:S(2)}) copy-start(bf16[2,4096,32]{1,2,0:T(8,128)(2,1)} %param.21) | copy-start | bytes 1572868
  104.7 2.0 collective-permute-start
  106.8 66.8 %copy-start.3 = (bf16[2,4096,256]{2,1,0:T(8,128)(2,1)S(1)}, bf16[2,4096,256]{2,1,0:T(8,128)(2,1)}, u32[]{:S(2)}) copy-start(bf16[2,4096,256]{2,1,0:T(8,128)(2,1)} %param.20) | copy-start | bytes 12582916
  106.8 14.6 %collective-permute-start.1 = (f32[32,4096]{1,0:T(8,128)S(1)}, f32[32,4096]{1,0:T(8,128)S(1)}, u32[]{:S(2)}, u32[]{:S(2)}) collective-permute-start(f32[32,4096]{1,0:T(8,128)S(1)} %add.167), channel_id=1, source_target_pairs={{0,2},{1,3},{2,0},{3,1},{4,6},{5,7},{6,4},{7,5},{8,10},{9,11},{10,... | collective-permute-start | bytes 1572872 | tf_op jit(solution)/shard_map/ppermute | solution.py:96
  121.4 52.6 %copy-start.7 = (bf16[2,4096,128]{2,1,0:T(8,128)(2,1)S(1)}, bf16[2,4096,128]{2,1,0:T(8,128)(2,1)}, u32[]{:S(2)}) copy-start(bf16[2,4096,128]{2,1,0:T(8,128)(2,1)} %param.23) | copy-start | bytes 6291460
  121.4 13.5 %collective-permute-start.2 = (f32[32,4096]{1,0:T(8,128)S(1)}, f32[32,4096]{1,0:T(8,128)S(1)}, u32[]{:S(2)}, u32[]{:S(2)}) collective-permute-start(f32[32,4096]{1,0:T(8,128)S(1)} %add.168), channel_id=1, source_target_pairs={{0,4},{1,5},{2,6},{3,7},{4,0},{5,1},{6,2},{7,3},{8,12},{9,13},{10,... | collective-permute-start | bytes 1572872 | tf_op jit(solution)/shard_map/ppermute | solution.py:96
  134.9 13.7 %collective-permute-start.3 = (f32[32,4096]{1,0:T(8,128)S(1)}, f32[32,4096]{1,0:T(8,128)S(1)}, u32[]{:S(2)}, u32[]{:S(2)}) collective-permute-start(f32[32,4096]{1,0:T(8,128)S(1)} %add.169), channel_id=1, source_target_pairs={{0,8},{1,9},{2,10},{3,11},{4,12},{5,13},{6,14},{7,15},{8,0},{9,1},... | collective-permute-start | bytes 1572872 | tf_op jit(solution)/shard_map/ppermute | solution.py:96
  148.7 24.2 %collective-permute-start.4 = (f32[32,4096]{1,0:T(8,128)S(1)}, f32[32,4096]{1,0:T(8,128)S(1)}, u32[]{:S(2)}, u32[]{:S(2)}) collective-permute-start(f32[32,4096]{1,0:T(8,128)S(1)} %add.170), channel_id=1, source_target_pairs={{0,16},{1,17},{2,18},{3,19},{4,20},{5,21},{6,22},{7,23},{8,24},{9,... | collective-permute-start | bytes 1572872 | tf_op jit(solution)/shard_map/ppermute | solution.py:96
  216.4 5.6 %copy-start.5 = (bf16[2,4096,256]{2,1,0:T(8,128)(2,1)S(1)}, bf16[2,4096,256]{2,1,0:T(8,128)(2,1)}, u32[]{:S(2)}) copy-start(bf16[2,4096,256]{2,1,0:T(8,128)(2,1)} %param.19) | copy-start | bytes 12582916
  261.9 1.9 collective-permute-start.5
  263.9 14.6 %collective-permute-start.6 = (f32[32,4096]{1,0:T(8,128)S(1)}, f32[32,4096]{1,0:T(8,128)S(1)}, u32[]{:S(2)}, u32[]{:S(2)}) collective-permute-start(f32[32,4096]{1,0:T(8,128)S(1)} %add.184), channel_id=1, source_target_pairs={{0,2},{1,3},{2,0},{3,1},{4,6},{5,7},{6,4},{7,5},{8,10},{9,11},{10,... | collective-permute-start | bytes 1572872 | tf_op jit(solution)/shard_map/ppermute | solution.py:96
  278.5 13.5 %collective-permute-start.7 = (f32[32,4096]{1,0:T(8,128)S(1)}, f32[32,4096]{1,0:T(8,128)S(1)}, u32[]{:S(2)}, u32[]{:S(2)}) collective-permute-start(f32[32,4096]{1,0:T(8,128)S(1)} %add.185), channel_id=1, source_target_pairs={{0,4},{1,5},{2,6},{3,7},{4,0},{5,1},{6,2},{7,3},{8,12},{9,13},{10,... | collective-permute-start | bytes 1572872 | tf_op jit(solution)/shard_map/ppermute | solution.py:96
  292.0 13.7 %collective-permute-start.8 = (f32[32,4096]{1,0:T(8,128)S(1)}, f32[32,4096]{1,0:T(8,128)S(1)}, u32[]{:S(2)}, u32[]{:S(2)}) collective-permute-start(f32[32,4096]{1,0:T(8,128)S(1)} %add.186), channel_id=1, source_target_pairs={{0,8},{1,9},{2,10},{3,11},{4,12},{5,13},{6,14},{7,15},{8,0},{9,1},... | collective-permute-start | bytes 1572872 | tf_op jit(solution)/shard_map/ppermute | solution.py:96
  305.8 24.2 %collective-permute-start.9 = (f32[32,4096]{1,0:T(8,128)S(1)}, f32[32,4096]{1,0:T(8,128)S(1)}, u32[]{:S(2)}, u32[]{:S(2)}) collective-permute-start(f32[32,4096]{1,0:T(8,128)S(1)} %add.187), channel_id=1, source_target_pairs={{0,16},{1,17},{2,18},{3,19},{4,20},{5,21},{6,22},{7,23},{8,24},{9,... | collective-permute-start | bytes 1572872 | tf_op jit(solution)/shard_map/ppermute | solution.py:96
